TPU v7x, 32 devices: a whole 2x2x4 slice. The times are simulated.
32 devices in a mesh: rep: 2 (over x), fs: 8 (over z, y), tp: 2 (over core).
Axes of the slice: x: 2, y: 2, z: 4, core: 2. Of those that a mesh axis runs over, the one named last changes fastest.
Arguments:
- tokens: bfloat16 [16, 384, 2048], P(('rep', 'fs')), may hold values from -6 to 6
- mix_gain: float32 [2048], replicated, may hold values from 0.1 to 1.9
- value_weight: float32 [2048, 2048], P('fs', 'tp'), may hold values from -0.125 to 0.125
- value_scale: float32 [2048], P(('tp', 'fs')), may hold values from 0.5 to 2
- inner_weight: float32 [2048, 2048], P('fs', 'tp'), may hold values from -0.125 to 0.125
- inner_scale: float32 [2048], P(('tp', 'fs')), may hold values from 0.5 to 2
- outer_weight: float32 [2048, 2048], P('fs', 'tp'), may hold values from -0.125 to 0.125
- outer_scale: float32 [2048], P(('tp', 'fs')), may hold values from 0.5 to 2
- conv_taps: float32 [3, 2048], P(None, 'tp'), may hold values from -3 to 3
- out_weight: float32 [2048, 2048], P('tp', 'fs'), may hold values from -0.125 to 0.125
- out_scale: float32 [2048], P('fs'), may hold values from 0.5 to 2
- mlp_gain: float32 [2048], replicated, may hold values from 0.1 to 1.9
- up_weight: float32 [2048, 6144], P('fs', 'tp'), may hold values from -0.125 to 0.125
- up_scale: float32 [6144], P(('tp', 'fs')), may hold values from 0.5 to 2
- down_weight: float32 [6144, 2048], P('tp', 'fs'), may hold values from -0.078125 to 0.078125
- down_scale: float32 [2048], P('fs'), may hold values from 0.5 to 2
Outputs:
- layer_out: bfloat16 [16, 384, 2048], P(('rep', 'fs'))
All inputs are finite; a program needn't handle non-finite values.
Results may differ from a plain program's by a relative error of at most 0.02.
Values may be sent and summed in bfloat16 or wider, within the bound.
A program may use at most 128 MiB of HBM per device.

v0:
```python
import jax
import jax.numpy as jnp
from jax import lax
from jax.sharding import PartitionSpec as P

norm_eps = 1e-06


def normalize(values, gain):
    return values * lax.rsqrt(jnp.mean(values * values, axis=-1, keepdims=True) + norm_eps) * gain


def add_rows(normed, piece):
    return jnp.dot(normed, piece, preferred_element_type=jnp.float32)


def body(
    tokens,
    mix_gain,
    value_weight,
    value_scale,
    inner_weight,
    inner_scale,
    outer_weight,
    outer_scale,
    conv_taps,
    out_weight,
    out_scale,
    mlp_gain,
    up_weight,
    up_scale,
    down_weight,
    down_scale,
):
    scales = (
        lax.all_gather(value_scale, "fs", axis=0, tiled=True),
        lax.all_gather(inner_scale, "fs", axis=0, tiled=True),
        lax.all_gather(outer_scale, "fs", axis=0, tiled=True),
        lax.all_gather(up_scale, "fs", axis=0, tiled=True),
        lax.all_gather(out_scale, "fs", axis=0, tiled=True),
        lax.all_gather(down_scale, "fs", axis=0, tiled=True),
    )
    value_cols, inner_cols, outer_cols, up_cols, out_cols, down_cols = scales
    start = tokens[0].astype(jnp.float32)
    normed = normalize(start, mix_gain).astype(jnp.bfloat16)
    value_b = value_weight.astype(jnp.bfloat16)
    inner_b = inner_weight.astype(jnp.bfloat16)
    outer_b = outer_weight.astype(jnp.bfloat16)

    def add_one(piece):
        return add_rows(normed, piece)

    value = add_one(lax.all_gather(value_b, "fs", axis=0, tiled=True))
    inner = add_one(lax.all_gather(inner_b, "fs", axis=0, tiled=True))
    outer = add_one(lax.all_gather(outer_b, "fs", axis=0, tiled=True))
    gated = inner * inner_cols * (value * value_cols)
    border = jnp.zeros((1, gated.shape[1]), jnp.float32)
    before = jnp.concatenate([border, gated[:-1]], axis=0)
    after = jnp.concatenate([gated[1:], border], axis=0)
    conv = conv_taps[0] * before + conv_taps[1] * gated + conv_taps[2] * after
    hidden = (outer * outer_cols * conv).astype(jnp.bfloat16)
    mix_part = jnp.dot(
        hidden,
        lax.all_gather(out_weight.astype(jnp.bfloat16), "fs", axis=1, tiled=True),
        preferred_element_type=jnp.float32,
    )
    mix_sum = lax.psum(mix_part.astype(jnp.bfloat16), "tp").astype(jnp.float32)
    middle = start + mix_sum * out_cols
    normed_mid = normalize(middle, mlp_gain).astype(jnp.bfloat16)
    up_b = up_weight.astype(jnp.bfloat16)
    down_b = down_weight.astype(jnp.bfloat16)
    upper = add_rows(normed_mid, lax.all_gather(up_b, "fs", axis=0, tiled=True))
    act = jnp.square(jax.nn.relu(upper * up_cols)).astype(jnp.bfloat16)
    mlp_part = jnp.dot(
        act, lax.all_gather(down_b, "fs", axis=1, tiled=True), preferred_element_type=jnp.float32
    )
    mlp_sum = lax.psum(mlp_part.astype(jnp.bfloat16), "tp").astype(jnp.float32)
    result = (middle + mlp_sum * down_cols).astype(jnp.bfloat16)
    return result[None]


def solution(mesh):
    placed = (
        P(("rep", "fs"), None, None),
        P(),
        P("fs", "tp"),
        P(("tp", "fs")),
        P("fs", "tp"),
        P(("tp", "fs")),
        P("fs", "tp"),
        P(("tp", "fs")),
        P(None, "tp"),
        P("tp", "fs"),
        P("fs"),
        P(),
        P("fs", "tp"),
        P(("tp", "fs")),
        P("tp", "fs"),
        P("fs"),
    )
    return jax.shard_map(
        body, mesh=mesh, in_specs=placed, out_specs=P(("rep", "fs"), None, None), check_vma=False
    )
```

profile of v0, /device:TPU:0, one launch (start us, length us, event | category | flops | bytes accessed | tf_op | source)
XLA Modules:
  0.0 739.5 jit_solution(12408413043940513878)
XLA Ops:
  6.5 2.2 convert_element_type.55
  8.8 2.2 convert_element_type.56
  12.1 2.1 convert_element_type.58
  14.3 22.8 %all-gather.1 = f32[8,1,128]{2,1,0:T(1,128)S(1)} all-gather(f32[1,1,128]{2,1,0:T(1,128)S(1)} %bitcast.51), channel_id=1, replica_groups=mesh['rep'=2,'fs'=8,'tp'=2] {'fs'}, dimensions={0}, use_global_device_ids=true | all-gather | bytes 4608 | tf_op jit(solution)/shard_map/all_gather | solution.py:37
  37.1 16.5 %all-gather.2 = f32[8,1,128]{2,1,0:T(1,128)S(1)} all-gather(f32[1,1,128]{2,1,0:T(1,128)S(1)} %bitcast.52), channel_id=1, replica_groups=mesh['rep'=2,'fs'=8,'tp'=2] {'fs'}, dimensions={0}, use_global_device_ids=true | all-gather | bytes 4608 | tf_op jit(solution)/shard_map/all_gather | solution.py:36
  53.6 19.0 %all-gather = f32[8,1,128]{2,1,0:T(1,128)S(1)} all-gather(f32[1,1,128]{2,1,0:T(1,128)S(1)} %bitcast.53), channel_id=1, replica_groups=mesh['rep'=2,'fs'=8,'tp'=2] {'fs'}, dimensions={0}, use_global_device_ids=true | all-gather | bytes 4608 | tf_op jit(solution)/shard_map/all_gather | solution.py:38
  73.0 12.1 %all-gather.15.cloned.1.call-done = bf16[2048,1024]{1,0:T(8,128)(2,1)} async-done(((bf16[256,1024]{1,0:T(8,128)(2,1)}), bf16[2048,1024]{1,0:T(8,128)(2,1)}) %all-gather.15.cloned.1.call-update) | async-done | bytes 4194320 | tf_op jit(solution)/shard_map/all_gather | solution.py:54
  85.1 5.2 fusion.11
  90.3 68.3 %all-gather.17.cloned.1.call-done = bf16[2048,1024]{1,0:T(8,128)(2,1)} async-done(((bf16[256,1024]{1,0:T(8,128)(2,1)}), bf16[2048,1024]{1,0:T(8,128)(2,1)}) %all-gather.17.cloned.1.call-update) | async-done | bytes 4194320 | tf_op jit(solution)/shard_map/all_gather | solution.py:53
  158.6 4.5 multiply_multiply_fusion
  163.1 2.0 fusion.15
  165.1 67.0 %all-gather.13.cloned.1.call-done = bf16[2048,1024]{1,0:T(8,128)(2,1)} async-done(((bf16[256,1024]{1,0:T(8,128)(2,1)}), bf16[2048,1024]{1,0:T(8,128)(2,1)}) %all-gather.13.cloned.1.call-update) | async-done | bytes 4194320 | tf_op jit(solution)/shard_map/all_gather | solution.py:55
  232.1 75.1 %all-gather.19.cloned.1.call-done = bf16[1024,2048]{1,0:T(8,128)(2,1)} async-done(((bf16[1024,256]{1,0:T(8,128)(2,1)}), bf16[1024,2048]{1,0:T(8,128)(2,1)}) %all-gather.19.cloned.1.call-update) | async-done | bytes 4194320 | tf_op jit(solution)/shard_map/all_gather | solution.py:64
  307.2 9.3 %convolution_convert_fusion = bf16[384,2048]{1,0:T(8,128)(2,1)} fusion(bf16[1024,2048]{1,0:T(8,128)(2,1)} %all-gather.19.cloned.1.call-done, f32[383,1024]{1,0:T(8,128)} %get-tuple-element.6, f32[384,1024]{1,0:T(8,128)S(1)} %multiply_multiply_fusion, f32[383,1024]{1,0:T(8,128)} %get-tuple-element.5, bf16[2048,1024]{1,0:T(8,128)(2,1)} %all-gather.13.cloned.1.call-done, ...), kind=kOutput, calls=%fused_computation.10 | convolution fusion | flops 3228303360 | bytes 16270848 | tf_op jit(solution)/shard_map/dot_general | solution.py:62
  316.5 3.3 convert_element_type.62
  320.0 3.6 convert_element_type.64
  323.7 17.8 %all-gather.3 = f32[8,1,256]{2,1,0:T(1,128)S(1)} all-gather(f32[1,1,256]{2,1,0:T(1,128)S(1)} %bitcast.49), channel_id=1, replica_groups=mesh['rep'=2,'fs'=8,'tp'=2] {'fs'}, dimensions={0}, use_global_device_ids=true | all-gather | bytes 9216 | tf_op jit(solution)/shard_map/all_gather | solution.py:40
  341.5 27.0 %all-gather.4 = f32[8,1,384]{2,1,0:T(1,128)S(1)} all-gather(f32[1,1,384]{2,1,0:T(1,128)S(1)} %reshape.35), channel_id=1, replica_groups=mesh['rep'=2,'fs'=8,'tp'=2] {'fs'}, dimensions={0}, use_global_device_ids=true | all-gather | bytes 13824 | tf_op jit(solution)/shard_map/all_gather | solution.py:39
  368.5 2.2 multiply_reduce_fusion
  370.7 143.9 %all-gather.21.cloned.1.call-done = bf16[2048,3072]{1,0:T(8,128)(2,1)} async-done(((bf16[256,3072]{1,0:T(8,128)(2,1)}), bf16[2048,3072]{1,0:T(8,128)(2,1)}) %all-gather.21.cloned.1.call-update) | async-done | bytes 12582928 | tf_op jit(solution)/shard_map/all_gather | solution.py:72
  514.7 176.4 %all-gather.23.cloned.1.call-done = bf16[3072,2048]{1,0:T(8,128)(2,1)} async-done(((bf16[3072,256]{1,0:T(8,128)(2,1)}), bf16[3072,2048]{1,0:T(8,128)(2,1)}) %all-gather.23.cloned.1.call-update) | async-done | bytes 12582928 | tf_op jit(solution)/shard_map/all_gather | solution.py:75
  691.0 19.4 %convolution_convert_fusion.1 = bf16[384,2048]{1,0:T(8,128)(2,1)} fusion(bf16[3072,2048]{1,0:T(8,128)(2,1)} %all-gather.23.cloned.1.call-done, bf16[2048,3072]{1,0:T(8,128)(2,1)} %all-gather.21.cloned.1.call-done, f32[3072]{0:T(1024)S(1)} %bitcast.42, bf16[384,2048]{1,0:T(8,128)(2,1)S(1)} %copy-done.1, bf16[1,384,2048]{2,1,0:T(8,128)(2,1)S(1)} %copy-done, ...), kind=kOutput, calls=%fused_computation.11 | convolution fusion | flops 9674686464 | bytes 29914624 | tf_op jit(solution)/shard_map/dot_general | solution.py:74
  710.5 17.7 %all-gather.5 = f32[8,1,256]{2,1,0:T(1,128)S(1)} all-gather(f32[1,1,256]{2,1,0:T(1,128)S(1)} %bitcast.50), channel_id=1, replica_groups=mesh['rep'=2,'fs'=8,'tp'=2] {'fs'}, dimensions={0}, use_global_device_ids=true | all-gather | bytes 9216 | tf_op jit(solution)/shard_map/all_gather | solution.py:41
  729.2 3.5 fusion.3
  (48 shorter events, 2.7 us)
Async XLA Ops:
  6.5 4.6 copy-start.2
  6.5 78.6 %all-gather.15.cloned.1.call-start = ((), (), s32[]{:S(2)}) async-start(), calls=%async_computation.1 | async-start | bytes 4718592 | tf_op jit(solution)/shard_map/all_gather | solution.py:54
  8.7 5.5 copy-start.7
  8.8 28.3 %copy-start.8 = (f32[128]{0:T(128)S(1)}, f32[128]{0:T(128)}, u32[]{:S(2)}) copy-start(f32[128]{0:T(128)} %param.19) | copy-start | bytes 1540
  8.8 44.8 %copy-start.9 = (f32[128]{0:T(128)S(1)}, f32[128]{0:T(128)}, u32[]{:S(2)}) copy-start(f32[128]{0:T(128)} %param.23) | copy-start | bytes 1540
  8.8 63.8 %copy-start = (bf16[1,384,2048]{2,1,0:T(8,128)(2,1)S(1)}, bf16[1,384,2048]{2,1,0:T(8,128)(2,1)}, u32[]{:S(2)}) copy-start(bf16[1,384,2048]{2,1,0:T(8,128)(2,1)} %param.16) | copy-start | bytes 4718596
  8.8 149.8 %all-gather.17.cloned.1.call-start = ((), (), s32[]{:S(2)}) async-start(), calls=%async_computation.2 | async-start | bytes 4718592 | tf_op jit(solution)/shard_map/all_gather | solution.py:53
  11.1 61.9 %copy-start.3 = (f32[3,1024]{1,0:T(4,128)S(1)}, f32[3,1024]{1,0:T(4,128)}, u32[]{:S(2)}) copy-start(f32[3,1024]{1,0:T(4,128)} %param.24) | copy-start | bytes 36868
  11.1 74.0 %copy-start.10 = (f32[2048]{0:T(1024)S(1)}, f32[2048]{0:T(1024)}, u32[]{:S(2)}) copy-start(f32[2048]{0:T(1024)} %param.17) | copy-start | bytes 24580
  11.1 221.0 %all-gather.13.cloned.1.call-start = ((), (), s32[]{:S(2)}) async-start(), calls=%async_computation | async-start | bytes 4718592 | tf_op jit(solution)/shard_map/all_gather | solution.py:55
  12.1 295.1 %all-gather.19.cloned.1.call-start = ((), (), s32[]{:S(2)}) async-start(), calls=%async_computation.3 | async-start | bytes 4718592 | tf_op jit(solution)/shard_map/all_gather | solution.py:64
  14.2 354.3 %all-reduce.5.cloned.1.call-start = ((), (), s32[]{:S(2)}) async-start(), calls=%async_computation.4 | async-start | bytes 3145728 | tf_op jit(solution)/shard_map/psum | solution.py:67
  316.5 198.2 %all-gather.21.cloned.1.call-start = ((), (), s32[]{:S(2)}) async-start(), calls=%async_computation.5 | async-start | bytes 14155776 | tf_op jit(solution)/shard_map/all_gather | solution.py:72
  319.9 3.8 copy-start.4
  319.9 3.8 copy-start.5
  319.9 371.1 %all-gather.23.cloned.1.call-start = ((), (), s32[]{:S(2)}) async-start(), calls=%async_computation.6 | async-start | bytes 14155776 | tf_op jit(solution)/shard_map/all_gather | solution.py:75
  323.6 367.5 %copy-start.11 = (f32[2048]{0:T(1024)S(1)}, f32[2048]{0:T(1024)}, u32[]{:S(2)}) copy-start(f32[2048]{0:T(1024)} %param.27) | copy-start | bytes 24580
  323.6 405.5 %all-reduce.7.cloned.1.call-start = ((), (), s32[]{:S(2)}) async-start(), calls=%async_computation.7 | async-start | bytes 3145728 | tf_op jit(solution)/shard_map/psum | solution.py:77
  368.5 322.5 %copy-start.1 = (bf16[384,2048]{1,0:T(8,128)(2,1)S(1)}, bf16[384,2048]{1,0:T(8,128)(2,1)}, u32[]{:S(2)}) copy-start(bf16[384,2048]{1,0:T(8,128)(2,1)} %all-reduce.5.cloned.1.call-done) | copy-start | bytes 4718596
  691.0 19.4 %copy-start.6 = (f32[256]{0:T(256)S(1)}, f32[256]{0:T(256)}, u32[]{:S(2)}) copy-start(f32[256]{0:T(256)} %param.31) | copy-start | bytes 3076
Sparse Core Ops, SparseCore 0:
  9.5 75.6 all-gather.14
  87.2 71.3 all-gather.16
  160.7 71.3 all-gather.12
  234.0 73.1 all-gather.18
  316.6 18.5 all-reduce.4
  337.2 177.3 all-gather.20
  516.7 174.2 all-gather.22
  710.6 18.5 all-reduce.6
where the time goes:
time: 740 us; the launch traced here: 739 us
  waiting for transfers between devices  544 us (74%)
  blocking collectives  121 us (16%)
  matrix products  38.3 us (5%)
  other arithmetic  20.4 us (3%)
  between operations  13.6 us (2%)
    all_gather x1, waiting for transfers between devices, body(): lax.all_gather(down_b, 'fs', axis=1, tiled=True)  176 us
    all_gather x1, waiting for transfers between devices, body(): upper = add_rows(normed_mid, lax.all_gather(up_b, 'fs', axis=0, tiled=True))  144 us
    all_gather x1, waiting for transfers between devices, body(): lax.all_gather(out_weight.astype(jnp.bfloat16), 'fs', axis=1, tiled=True)  75.1 us
    all_gather x1, waiting for transfers between devices, body(): value = add_one(lax.all_gather(value_b, 'fs', axis=0, tiled=True))  68.3 us
    all_gather x1, waiting for transfers between devices, body(): outer = add_one(lax.all_gather(outer_b, 'fs', axis=0, tiled=True))  67 us
    all_gather x1, blocking collectives, body(): lax.all_gather(up_scale, 'fs', axis=0, tiled=True)  27 us
    all_gather x1, blocking collectives, body(): lax.all_gather(inner_scale, 'fs', axis=0, tiled=True)  22.8 us
    dot_general x1, matrix products, body(): jnp.dot(act, lax.all_gather(down_b, 'fs', axis=1, tiled=True), preferred_...  19.4 us
  transfers between devices with their start and end apart: 8, of which 7 were waited for; matrix products, arithmetic and copies ran while one was open for 4% of the time, Pallas kernels for 0%

commit v1 on v0

v1 whole, which is shorter than its diff:
```python
import functools

import jax
import jax.numpy as jnp
from jax import lax
from jax.experimental import pallas as pl
from jax.experimental.pallas import tpu as pltpu
from jax.sharding import PartitionSpec as P

MESH = pl.DeviceIdType.MESH
norm_eps = 1e-06
HALO = 16
TILE = 16
f32 = jnp.float32
bf16 = jnp.bfloat16


def kernel(
    nz, G, T, win, rows,
    tok, g1, g2, asc, taps, usc, oc, dc, wa, wo, wu, wd,
    out,
    WA, WO, WU, WD, nrm, hid, p1, q1, mid32, mid, act, p2, q2,
    rz, rd, sz, sd, sy, loc, rn, sn, r1, s1, ra, sa, r2, s2, ro, so,
):
    D = tok.shape[1]
    pw = D // nz
    cw = pw // 2
    r, f, t = lax.axis_index("rep"), lax.axis_index("fs"), lax.axis_index("tp")
    z, y = f // 2, f % 2
    fy = z * 2 + 1 - y
    g = r * 2 + y
    srcs = (wa, wo, wu, wd)
    ka, ko, ku, kd = (w.shape[1] for w in srcs)
    has_lo, has_hi = z > 0, z < nz - 1
    if T == 2:
        start, off = t * (rows - HALO), t * HALO
    else:
        start = jnp.clip(t * rows - HALO, 0, tok.shape[0] - win)
        off = t * rows - start
    start, off = pl.multiple_of(start, HALO), pl.multiple_of(off, HALO)

    def member(m):
        return (m // 2, z * 2 + m % 2, t)

    def others():
        return [(g + d) % G for d in range(1, G)]

    def siblings():
        return [(t + d) % T for d in range(1, T)]

    def copy(src, dst, ssem, rsem, dev):
        return pltpu.make_async_remote_copy(
            src_ref=src, dst_ref=dst, send_sem=ssem, recv_sem=rsem, device_id=dev, device_id_type=MESH
        )

    def arrived(ref, sem):
        pltpu.make_async_copy(ref, ref, sem).wait()

    def slot(s, ff, tt):
        if s == 0:
            return WA.at[tt, pl.ds(pl.multiple_of(ff * ka, ka), ka)]
        if s == 1:
            return WO.at[ff, pl.ds(pl.multiple_of(tt * ko, ko), ko)]
        if s == 2:
            return WU.at[tt, pl.ds(pl.multiple_of(ff * ku, ku), ku)]
        return WD.at[ff, pl.ds(pl.multiple_of(tt * kd, kd), kd)]

    def to_siblings(s, ff, src):
        for tt in siblings():
            copy(src, slot(s, ff, t), sd.at[s, ff], rd.at[s, ff], (r, f, tt)).start()

    def both_ways(s, ff, src):
        @pl.when(has_lo)
        def _():
            copy(src, slot(s, ff, t), sz.at[s, ff, 0], rz.at[s, ff], (r, f - 2, t)).start()

        @pl.when(has_hi)
        def _():
            copy(src, slot(s, ff, t), sz.at[s, ff, 1], rz.at[s, ff], (r, f + 2, t)).start()

    def kick(s):
        own = srcs[s]
        copy(own.at[1 - y], slot(s, f, t), sy.at[s], rz.at[s, f], (r, fy, t)).start()
        pltpu.make_async_copy(own.at[y], slot(s, f, t), loc.at[s]).start()
        both_ways(s, f, own.at[y])
        to_siblings(s, f, own.at[y])

    def kick2(s):
        arrived(slot(s, fy, t), rz.at[s, fy])
        both_ways(s, fy, slot(s, fy, t))
        to_siblings(s, fy, slot(s, fy, t))

    def place(j):
        k = (j + 1) // 2
        sg = 1 - 2 * (j % 2)
        return z + sg * k, z - sg

    def step(s, j):
        zs, nxt = place(j)

        @pl.when(jnp.logical_and(zs >= 0, zs < nz))
        def _():
            for yy in range(2):
                ff = 2 * zs + yy
                arrived(slot(s, ff, t), rz.at[s, ff])

                @pl.when(jnp.logical_and(nxt >= 0, nxt < nz))
                def _():
                    copy(
                        slot(s, ff, t), slot(s, ff, t), sz.at[s, ff, 0], rz.at[s, ff], (r, 2 * nxt + y, t)
                    ).start()

                to_siblings(s, ff, slot(s, ff, t))

    def steps(s, lo, hi):
        @pl.loop(lo, hi)
        def _(j):
            step(s, j)

    def from_siblings(s, ff):
        for tt in siblings():
            arrived(slot(s, ff, tt), rd.at[s, ff])

    def all_from_siblings(s):
        arrived(slot(s, f, t), loc.at[s])

        @pl.loop(0, 2 * nz)
        def _(ff):
            from_siblings(s, ff)

    last = 2 * nz - 1

    barrier = pltpu.get_barrier_semaphore()
    for m in others():
        pl.semaphore_signal(barrier, inc=1, device_id=member(m), device_id_type=MESH)
    for tt in siblings():
        pl.semaphore_signal(barrier, inc=1, device_id=(r, f, tt), device_id_type=MESH)

    @pl.when(has_lo)
    def _():
        pl.semaphore_signal(barrier, inc=1, device_id=(r, f - 2, t), device_id_type=MESH)

    @pl.when(has_hi)
    def _():
        pl.semaphore_signal(barrier, inc=1, device_id=(r, f + 2, t), device_id_type=MESH)

    pl.semaphore_wait(barrier, G + T - 2 + (z + nz - 1) // nz + (2 * nz - 2 - z) // nz)

    kick(0)
    kick(1)

    @pl.loop(0, win // TILE)
    def _(i):
        at = pl.ds(pl.multiple_of(i * TILE, TILE), TILE)
        x = tok[pl.ds(pl.multiple_of(start + i * TILE, TILE), TILE), :].astype(f32)
        x = x * lax.rsqrt(jnp.mean(x * x, axis=-1, keepdims=True) + norm_eps) * g1[...]
        nrm[g, at, :] = x.astype(bf16)

    kick2(0)
    for m in others():
        copy(nrm.at[g], nrm.at[g], sn.at[m], rn.at[g], member(m)).start()
    kick(2)
    kick2(1)
    steps(0, 1, last)
    kick(3)
    kick2(2)
    steps(1, 1, last)

    all_from_siblings(0)
    for m in others():
        arrived(nrm.at[m], rn.at[m])
    c = taps.shape[2]

    @pl.loop(0, G)
    def _(gs):
        x = nrm[gs]
        row = lax.broadcasted_iota(jnp.int32, (win, c), 0)
        for tt in range(T):
            prod = jnp.dot(x, WA[tt], preferred_element_type=f32) * asc[tt]
            gated = prod[:, c : 2 * c] * prod[:, :c]
            before = jnp.where(row == 0, 0.0, pltpu.roll(gated, 1, 0))
            after = jnp.where(row == win - 1, 0.0, pltpu.roll(gated, win - 1, 0))
            conv = taps[tt, 0:1] * before + taps[tt, 1:2] * gated + taps[tt, 2:3] * after
            hid[gs, :, tt * c : (tt + 1) * c] = (prod[:, 2 * c :] * conv).astype(bf16)

    all_from_siblings(1)

    @pl.loop(0, nz)
    def _(zs):
        @pl.loop(0, G)
        def _(gs):
            h = hid[gs, pl.ds(off, rows), :]
            for yy in range(2):
                p1[gs, zs, :, yy * cw : (yy + 1) * cw] = jnp.dot(
                    h, WO[2 * zs + yy], preferred_element_type=f32
                ).astype(bf16)

    kick2(3)
    for m in others():
        copy(p1.at[m], q1.at[g], s1.at[m], r1.at[g], member(m)).start()
    cut = (2 * last) // 3
    steps(2, 1, cut)

    for m in others():
        arrived(q1.at[m], r1.at[m])

    def total(p, q, zs, at):
        acc = p[g, zs, at, :].astype(f32)
        for m in others():
            acc = acc + q[m, zs, at, :].astype(f32)
        return acc

    @pl.loop(0, rows // TILE)
    def _(i):
        at = pl.ds(pl.multiple_of(i * TILE, TILE), TILE)
        here = pl.ds(pl.multiple_of(t * rows + i * TILE, TILE), TILE)
        ssq = jnp.zeros((TILE, 1), f32)
        for zs in range(nz):
            m = tok[here, zs * pw : (zs + 1) * pw].astype(f32) + total(p1, q1, zs, at) * oc[zs]
            mid32[zs, at, :] = m
            ssq = ssq + jnp.sum(m * m, axis=-1, keepdims=True)
        inv = lax.rsqrt(ssq / D + norm_eps)
        for zs in range(nz):
            cols = slice(zs * pw, (zs + 1) * pw)
            mid[g, at, cols] = (mid32[zs, at, :] * inv * g2[:, cols]).astype(bf16)

    steps(2, cut, cut + 1)
    for m in others():
        copy(mid.at[g], mid.at[g], sa.at[m], ra.at[g], member(m)).start()
    steps(2, cut + 1, last)
    cut2 = (last + 1) // 2
    steps(3, 1, cut2)

    all_from_siblings(2)
    for m in others():
        arrived(mid.at[m], ra.at[m])
    u = usc.shape[2]

    @pl.loop(0, G)
    def _(gs):
        x = mid[gs]
        for tt in range(T):
            upper = jnp.dot(x, WU[tt], preferred_element_type=f32) * usc[tt]
            act[gs, :, tt * u : (tt + 1) * u] = jnp.square(jnp.maximum(upper, 0.0)).astype(bf16)

    arrived(slot(3, f, t), loc.at[3])

    def down(j):
        zs, _ = place(j)

        @pl.when(jnp.logical_and(zs >= 0, zs < nz))
        def _():
            for yy in range(2):
                from_siblings(3, 2 * zs + yy)

            @pl.loop(0, G)
            def _(gs):
                x = act[gs]
                for yy in range(2):
                    p2[gs, zs, :, yy * cw : (yy + 1) * cw] = jnp.dot(
                        x, WD[2 * zs + yy], preferred_element_type=f32
                    ).astype(bf16)

            for m in others():
                copy(p2.at[m, zs], q2.at[g, zs], s2.at[m, zs], r2.at[g, zs], member(m)).start()

    @pl.loop(0, last)
    def _(j):
        @pl.when(j >= cut2)
        def _():
            step(3, j)

        down(j)

    @pl.loop(0, nz)
    def _(zs):
        for m in others():
            arrived(q2.at[m, zs], r2.at[m, zs])

    @pl.loop(0, rows // TILE)
    def _(i):
        at = pl.ds(pl.multiple_of(i * TILE, TILE), TILE)
        here = pl.ds(pl.multiple_of(t * rows + i * TILE, TILE), TILE)
        for zs in range(nz):
            out[here, zs * pw : (zs + 1) * pw] = (
                mid32[zs, at, :] + total(p2, q2, zs, at) * dc[zs]
            ).astype(bf16)

    def half(tt):
        return out.at[pl.ds(pl.multiple_of(tt * rows, rows), rows)]

    for tt in siblings():
        copy(half(t), half(t), so.at[tt], ro.at[t], (r, f, tt)).start()

    for s in range(4):
        own = srcs[s].at[y]
        arrived(own, sy.at[s])

        def gone(ff, k, s=s, own=own):
            arrived(own, sz.at[s, ff, k])

        for ff in (f, fy):
            pl.when(has_lo)(functools.partial(gone, ff, 0))
            pl.when(has_hi)(functools.partial(gone, ff, 1))

        @pl.loop(1, last)
        def _(j):
            zs, nxt = place(j)
            ok = jnp.logical_and(zs >= 0, zs < nz)

            @pl.when(jnp.logical_and(ok, jnp.logical_and(nxt >= 0, nxt < nz)))
            def _():
                for yy in range(2):
                    gone(2 * zs + yy, 0)

        @pl.loop(0, 2 * nz)
        def _(ff):
            for _ in siblings():
                arrived(own, sd.at[s, ff])

    for m in others():
        arrived(nrm.at[m], sn.at[m])
        arrived(p1.at[m], s1.at[m])
        arrived(mid.at[m], sa.at[m])

        @pl.loop(0, nz)
        def _(zs):
            arrived(p2.at[m, zs], s2.at[m, zs])

    for tt in siblings():
        arrived(half(tt), ro.at[tt])
        arrived(half(tt), so.at[tt])


def body(
    R, n_fs, T,
    tokens, mix_gain, value_weight, value_scale, inner_weight, inner_scale, outer_weight, outer_scale,
    conv_taps, out_weight, out_scale, mlp_gain, up_weight, up_scale, down_weight, down_scale,
):
    G, nz = 2 * R, n_fs // 2
    TOK, D = tokens.shape[1:]
    rows = TOK // T
    win = TOK if T == 1 else rows + HALO if T == 2 else rows + 2 * HALO
    r, f = lax.axis_index("rep"), lax.axis_index("fs")
    g = r * 2 + f % 2

    vs, us, os = value_scale.shape[0], up_scale.shape[0], out_scale.shape[0]
    tap = lax.dynamic_slice_in_dim(conv_taps, f * vs, vs, axis=1)
    packed = jnp.concatenate(
        [value_scale, inner_scale, outer_scale, tap[0], tap[1], tap[2], up_scale, out_scale, down_scale]
    )
    every = lax.all_gather(packed, ("tp", "fs"), axis=0, tiled=False).reshape(T, n_fs, -1)

    def block(v):
        return lax.dynamic_index_in_dim(v.reshape(T, G, -1), g, axis=1, keepdims=True)

    small = [block(every[:, :, i * vs : (i + 1) * vs]) for i in range(6)]
    asc = jnp.concatenate(small[:3], axis=2)
    taps = jnp.concatenate(small[3:], axis=1)
    usc = block(every[:, :, 6 * vs : 6 * vs + us])
    oc = every[0, :, 6 * vs + us : 6 * vs + us + os].reshape(nz, 1, -1)
    dc = every[0, :, 6 * vs + us + os :].reshape(nz, 1, -1)

    def col_blocks(w):
        w = lax.dynamic_index_in_dim(w.reshape(w.shape[0], R, -1), r, axis=1, keepdims=False)
        return w.reshape(w.shape[0], 2, -1).swapaxes(0, 1).astype(bf16)

    def row_blocks(w):
        w = lax.dynamic_index_in_dim(w.reshape(R, -1, w.shape[1]), r, axis=0, keepdims=False)
        return w.reshape(2, -1, w.shape[1]).astype(bf16)

    wa = jnp.concatenate([col_blocks(value_weight), col_blocks(inner_weight), col_blocks(outer_weight)], axis=2)
    wo, wu, wd = row_blocks(out_weight), col_blocks(up_weight), row_blocks(down_weight)
    ko, kd = wo.shape[1], wd.shape[1]
    pw = D // nz
    dma = pltpu.SemaphoreType.DMA
    vmem = pl.BlockSpec(memory_space=pltpu.VMEM)
    hbm = pl.BlockSpec(memory_space=pl.ANY)
    result = pl.pallas_call(
        functools.partial(kernel, nz, G, T, win, rows),
        out_shape=jax.ShapeDtypeStruct((TOK, D), bf16),
        in_specs=[vmem] * 8 + [hbm] * 4,
        out_specs=vmem,
        scratch_shapes=[
            pltpu.VMEM((T, D, wa.shape[2]), bf16),
            pltpu.VMEM((n_fs, T * ko, wo.shape[2]), bf16),
            pltpu.VMEM((T, D, wu.shape[2]), bf16),
            pltpu.VMEM((n_fs, T * kd, wd.shape[2]), bf16),
            pltpu.VMEM((G, win, D), bf16),
            pltpu.VMEM((G, win, T * ko), bf16),
            pltpu.VMEM((G, nz, rows, pw), bf16),
            pltpu.VMEM((G, nz, rows, pw), bf16),
            pltpu.VMEM((nz, rows, pw), f32),
            pltpu.VMEM((G, rows, D), bf16),
            pltpu.VMEM((G, rows, T * kd), bf16),
            pltpu.VMEM((G, nz, rows, pw), bf16),
            pltpu.VMEM((G, nz, rows, pw), bf16),
            dma((4, n_fs)),
            dma((4, n_fs)),
            dma((4, n_fs, 2)),
            dma((4, n_fs)),
            dma((4,)),
            dma((4,)),
            dma((G,)),
            dma((G,)),
            dma((G,)),
            dma((G,)),
            dma((G,)),
            dma((G,)),
            dma((G, nz)),
            dma((G, nz)),
            dma((T,)),
            dma((T,)),
        ],
        compiler_params=pltpu.CompilerParams(
            collective_id=0, has_side_effects=True, vmem_limit_bytes=65000000
        ),
    )(tokens[0], mix_gain[None], mlp_gain[None], asc, taps, usc, oc, dc, wa, wo, wu, wd)
    return result[None]


def solution(mesh):
    placed = (
        P(("rep", "fs"), None, None),
        P(),
        P("fs", "tp"),
        P(("tp", "fs")),
        P("fs", "tp"),
        P(("tp", "fs")),
        P("fs", "tp"),
        P(("tp", "fs")),
        P(None, "tp"),
        P("tp", "fs"),
        P("fs"),
        P(),
        P("fs", "tp"),
        P(("tp", "fs")),
        P("tp", "fs"),
        P("fs"),
    )
    sizes = (mesh.shape["rep"], mesh.shape["fs"], mesh.shape["tp"])
    return jax.shard_map(
        functools.partial(body, *sizes),
        mesh=mesh,
        in_specs=placed,
        out_specs=P(("rep", "fs"), None, None),
        check_vma=False,
    )
```

time: 740 us -> 285 us (0.39)
  waiting for transfers between devices: 544 us -> 0 us
  Pallas kernels: 0 us -> 227 us
  blocking collectives: 121 us -> 34.8 us
  matrix products: 38.3 us -> 0 us
  other arithmetic: 20.4 us -> 2.13 us
  local copies, waits for them, and re-layouts: 2.06 us -> 20 us
  between operations: 13.6 us -> 0.17 us
    all_gather x6 -> x0, waiting for transfers between devices: 543 us -> none  [the longest x1 176 us: body(): lax.all_gather(down_b, 'fs', axis=1, tiled=True)]
    pallas_call x0 -> x1, Pallas kernels: none -> 227 us  [body(): pl.pallas_call(functools.partial(kernel, nz, G, T, win, rows), out_shape=...]
    all_gather x6 -> x1, blocking collectives: 121 us -> 34.8 us  [body(): lax.all_gather(packed, ('tp', 'fs'), axis=0, tiled=False)]
    dot_general x4 -> x0, matrix products: 38.3 us -> none  [the longest x1 19.4 us: body(): jnp.dot(act, lax.all_gather(down_b, 'fs', axis=1, tiled=True), preferred_...]
    convert_element_type x6 -> x0, other arithmetic: 14.3 us -> none  [the longest x1 3.61 us: body(): down_b = down_weight.astype(jnp.bfloat16)]
    unnamed x25 -> x21, local copies, waits for them, and re-layouts: 0.06 us -> 10.1 us
  transfers between devices with their start and end apart: 8 -> 0, of which waited for: 7 -> 0; matrix products, arithmetic and copies ran while one was open for 4% -> 0% of each run, Pallas kernels for 0% -> 0%
where the time goes in v1:
time: 285 us; the launch traced here: 284 us
  Pallas kernels  227 us (80%)
  blocking collectives  34.8 us (12%)
  local copies, waits for them, and re-layouts  20 us (7%)
    pallas_call x1, Pallas kernels, body(): pl.pallas_call(functools.partial(kernel, nz, G, T, win, rows), out_shape=...  227 us
    all_gather x1, blocking collectives, body(): lax.all_gather(packed, ('tp', 'fs'), axis=0, tiled=False)  34.8 us
    unnamed x21, local copies, waits for them, and re-layouts  10.1 us

profile of v1, /device:TPU:0, one launch (start us, length us, event | category | flops | bytes accessed | tf_op | source)
XLA Modules:
  0.0 284.2 jit_solution(4514011685756809841)
XLA Ops:
  0.0 0.8 constant_dynamic-slice_fusion.7
  0.8 0.7 constant_dynamic-update-slice_fusion.8
  1.5 0.7 constant_dynamic-update-slice_fusion.7
  2.2 0.7 constant_dynamic-update-slice_fusion.6
  2.9 0.7 constant_dynamic-update-slice_fusion.2
  3.5 0.7 constant_dynamic-update-slice_fusion.1
  4.2 0.7 constant_dynamic-update-slice_fusion
  4.9 34.8 %all-gather.1 = f32[16,1,1664]{2,1,0:T(1,128)S(1)} all-gather(f32[1,1,1664]{2,1,0:T(1,128)S(1)} %reshape.76), channel_id=2, replica_groups=mesh['rep'=2,'fs'=8,'tp'=2] {'tp','fs'}, dimensions={0}, use_global_device_ids=true | all-gather | bytes 113152 | tf_op jit(solution)/shard_map/all_gather | solution.py:352
  39.8 0.6 constant_dynamic-slice_fusion.usc
  40.5 0.6 pad_maximum_fusion.1.taps
  41.1 0.6 pad_maximum_fusion.2.asc
  41.7 0.6 reshape_squeeze.6.oc
  42.3 0.6 reshape_squeeze.7.dc
  42.9 1.4 copy.29
  44.4 0.2 copy.27
  44.6 0.7 dynamic-slice_convert_fusion.3
  45.5 1.1 copy.30
  46.9 0.9 pad_maximum_fusion.wa
  47.9 2.2 copy.31
  50.1 1.2 copy.32
  51.3 2.4 dynamic-slice_convert_fusion
  53.6 0.7 dynamic-slice_convert_fusion.2
  54.4 227.1 %shard_map.154 = bf16[384,2048]{1,0:T(8,128)(2,1)} custom-call(bf16[384,2048]{1,0:T(8,128)(2,1)} %bitcast.35, f32[1,2048]{1,0:T(1,128)} %bitcast.50, f32[1,2048]{1,0:T(1,128)} %bitcast.51, f32[2,1,768]{2,1,0:T(1,128)} %pad_maximum_fusion.2.asc, f32[2,3,256]{2,1,0:T(4,128)} %pad_maximum_fusion.1.taps, f32[2,1,768]{2,1,0:T(1,128)} %constant_dynamic-slice_fusion.usc, ...), custom_call_target="tpu_custom_call" | custom-call | tf_op jit(solution)/shard_map/pallas_call | solution.py:379
  281.5 2.7 copy.46
  (30 shorter events, 0.7 us)
Async XLA Ops:
  0.0 53.6 %copy-start = (f32[1024,256]{1,0:T(8,128)S(1)}, f32[1024,256]{1,0:T(8,128)}, u32[]{:S(2)}) copy-start(f32[1024,256]{1,0:T(8,128)} %param.25) | copy-start | bytes 3145732
  0.0 44.3 %copy-start.1 = (f32[256,1024]{1,0:T(8,128)S(1)}, f32[256,1024]{1,0:T(8,128)}, u32[]{:S(2)}) copy-start(f32[256,1024]{1,0:T(8,128)} %param.20) | copy-start | bytes 3145732
  44.6 2.0 copy-start.2

commit v2 on v1

--- a/solution.py
+++ b/solution.py
@@ -16,12 +16,17 @@
 
 
 def kernel(
-    nz, G, T, win, rows,
-    tok, g1, g2, asc, taps, usc, oc, dc, wa, wo, wu, wd,
+    nz, G, T, win, rows, inside,
+    tok, g1, g2, vectors, weights,
     out,
     WA, WO, WU, WD, nrm, hid, p1, q1, mid32, mid, act, p2, q2,
+    staged, leaving, gathered,
     rz, rd, sz, sd, sy, loc, rn, sn, r1, s1, ra, sa, r2, s2, ro, so,
 ):
+    if inside:
+        packed, table, asc, taps, usc, oc, dc = gathered
+    else:
+        asc, taps, usc, oc, dc = vectors
     D = tok.shape[1]
     pw = D // nz
     cw = pw // 2
@@ -29,8 +34,8 @@
     z, y = f // 2, f % 2
     fy = z * 2 + 1 - y
     g = r * 2 + y
-    srcs = (wa, wo, wu, wd)
-    ka, ko, ku, kd = (w.shape[1] for w in srcs)
+    ka, ko, ku, kd = (w.shape[0] for w in leaving)
+    stages = range(5 if inside else 4)
     has_lo, has_hi = z > 0, z < nz - 1
     if T == 2:
         start, off = t * (rows - HALO), t * HALO
@@ -63,7 +68,9 @@
             return WO.at[ff, pl.ds(pl.multiple_of(tt * ko, ko), ko)]
         if s == 2:
             return WU.at[tt, pl.ds(pl.multiple_of(ff * ku, ku), ku)]
-        return WD.at[ff, pl.ds(pl.multiple_of(tt * kd, kd), kd)]
+        if s == 3:
+            return WD.at[ff, pl.ds(pl.multiple_of(tt * kd, kd), kd)]
+        return table.at[ff, tt]
 
     def to_siblings(s, ff, src):
         for tt in siblings():
@@ -78,12 +85,54 @@
         def _():
             copy(src, slot(s, ff, t), sz.at[s, ff, 1], rz.at[s, ff], (r, f + 2, t)).start()
 
+    def fetches():
+        for i, w in enumerate(weights):
+            src, dst = weights[i], staged[i]
+            if w.shape[1] > dst.shape[1]:
+                n = dst.shape[1]
+                src = src.at[:, pl.ds(pl.multiple_of(r * n, n), n)]
+            elif w.shape[0] > dst.shape[0]:
+                n = dst.shape[0]
+                src = src.at[pl.ds(pl.multiple_of(r * n, n), n)]
+            yield pltpu.make_async_copy(src, dst, loc.at[i])
+
+    def round_stage(s):
+        parts = {0: (0, 1, 2), 1: (3,), 2: (4,), 3: (5,)}[s]
+        high = leaving[s].shape[0]
+        for i in parts:
+            pltpu.make_async_copy(staged[i], staged[i], loc.at[i]).wait()
+        for yy in range(2):
+
+            @pl.when(y == yy)
+            def _():
+                @pl.loop(0, high // 32)
+                def _(k):
+                    at = pl.ds(pl.multiple_of(k * 32, 32), 32)
+                    for n, i in enumerate(parts):
+                        if s in (0, 2):
+                            wide = staged[i].shape[1] // 2
+                            mine = staged[i][at, yy * wide : (yy + 1) * wide]
+                            theirs = staged[i][at, (1 - yy) * wide : (2 - yy) * wide]
+                        else:
+                            wide = staged[i].shape[1]
+                            mine = staged[i][pl.ds(pl.multiple_of(yy * high + k * 32, 32), 32), :]
+                            theirs = staged[i][pl.ds(pl.multiple_of((1 - yy) * high + k * 32, 32), 32), :]
+                        cols = slice(n * wide, (n + 1) * wide)
+                        leaving[s][at, cols] = theirs.astype(bf16)
+                        if s == 0:
+                            WA[t, pl.ds(pl.multiple_of(f * ka + k * 32, 32), 32), cols] = mine.astype(bf16)
+                        elif s == 1:
+                            WO[f, pl.ds(pl.multiple_of(t * ko + k * 32, 32), 32), :] = mine.astype(bf16)
+                        elif s == 2:
+                            WU[t, pl.ds(pl.multiple_of(f * ku + k * 32, 32), 32), :] = mine.astype(bf16)
+                        else:
+                            WD[f, pl.ds(pl.multiple_of(t * kd + k * 32, 32), 32), :] = mine.astype(bf16)
+
     def kick(s):
-        own = srcs[s]
-        copy(own.at[1 - y], slot(s, f, t), sy.at[s], rz.at[s, f], (r, fy, t)).start()
-        pltpu.make_async_copy(own.at[y], slot(s, f, t), loc.at[s]).start()
-        both_ways(s, f, own.at[y])
-        to_siblings(s, f, own.at[y])
+        own = slot(s, f, t)
+        copy(leaving[s] if s < 4 else own, own, sy.at[s], rz.at[s, f], (r, fy, t)).start()
+        both_ways(s, f, own)
+        to_siblings(s, f, own)
 
     def kick2(s):
         arrived(slot(s, fy, t), rz.at[s, fy])
@@ -122,14 +171,28 @@
             arrived(slot(s, ff, tt), rd.at[s, ff])
 
     def all_from_siblings(s):
-        arrived(slot(s, f, t), loc.at[s])
-
         @pl.loop(0, 2 * nz)
         def _(ff):
             from_siblings(s, ff)
 
     last = 2 * nz - 1
 
+    for fetch in fetches():
+        fetch.start()
+    if inside:
+        at_col = 0
+        for v in vectors[:3]:
+            packed[:, at_col : at_col + v.shape[1]] = v[...]
+            at_col += v.shape[1]
+        few = vectors[0].shape[1]
+        for k in range(3):
+            packed[:, at_col : at_col + few] = vectors[6][k : k + 1, pl.ds(pl.multiple_of(f * few, few), few)]
+            at_col += few
+        for v in vectors[3:6]:
+            packed[:, at_col : at_col + v.shape[1]] = v[...]
+            at_col += v.shape[1]
+        table[f, t] = packed[...]
+
     barrier = pltpu.get_barrier_semaphore()
     for m in others():
         pl.semaphore_signal(barrier, inc=1, device_id=member(m), device_id_type=MESH)
@@ -146,8 +209,14 @@
 
     pl.semaphore_wait(barrier, G + T - 2 + (z + nz - 1) // nz + (2 * nz - 2 - z) // nz)
 
+    round_stage(0)
+    round_stage(1)
     kick(0)
+    if inside:
+        kick(4)
     kick(1)
+    round_stage(2)
+    round_stage(3)
 
     @pl.loop(0, win // TILE)
     def _(i):
@@ -157,11 +226,15 @@
         nrm[g, at, :] = x.astype(bf16)
 
     kick2(0)
+    if inside:
+        kick2(4)
     for m in others():
         copy(nrm.at[g], nrm.at[g], sn.at[m], rn.at[g], member(m)).start()
     kick(2)
     kick2(1)
     steps(0, 1, last)
+    if inside:
+        steps(4, 1, last)
     kick(3)
     kick2(2)
     steps(1, 1, last)
@@ -169,6 +242,25 @@
     all_from_siblings(0)
     for m in others():
         arrived(nrm.at[m], rn.at[m])
+    if inside:
+        all_from_siblings(4)
+        few, ups, outs = vectors[0].shape[1], vectors[3].shape[1], vectors[4].shape[1]
+        wide = 3 * vectors[0].shape[1] * 2
+        near = 2 * nz // G
+        for tt in range(T):
+            for j in range(near):
+                row_of = table[g * near + j, tt]
+                for k in range(3):
+                    at_col = (k * near + j) * few
+                    asc[tt, :, at_col : at_col + few] = row_of[:, k * few : (k + 1) * few]
+                    taps[tt, k : k + 1, j * few : (j + 1) * few] = row_of[:, (3 + k) * few : (4 + k) * few]
+                usc[tt, :, j * ups : (j + 1) * ups] = row_of[:, wide : wide + ups]
+        for zs in range(nz):
+            for yy in range(2):
+                row_of = table[2 * zs + yy, 0]
+                cols = slice(yy * outs, (yy + 1) * outs)
+                oc[zs, :, cols] = row_of[:, wide + ups : wide + ups + outs]
+                dc[zs, :, cols] = row_of[:, wide + ups + outs :]
     c = taps.shape[2]
 
     @pl.loop(0, G)
@@ -243,8 +335,6 @@
             upper = jnp.dot(x, WU[tt], preferred_element_type=f32) * usc[tt]
             act[gs, :, tt * u : (tt + 1) * u] = jnp.square(jnp.maximum(upper, 0.0)).astype(bf16)
 
-    arrived(slot(3, f, t), loc.at[3])
-
     def down(j):
         zs, _ = place(j)
 
@@ -292,8 +382,8 @@
     for tt in siblings():
         copy(half(t), half(t), so.at[tt], ro.at[t], (r, f, tt)).start()
 
-    for s in range(4):
-        own = srcs[s].at[y]
+    for s in stages:
+        own = slot(s, f, t)
         arrived(own, sy.at[s])
 
         def gone(ff, k, s=s, own=own):
@@ -345,47 +435,52 @@
     g = r * 2 + f % 2
 
     vs, us, os = value_scale.shape[0], up_scale.shape[0], out_scale.shape[0]
-    tap = lax.dynamic_slice_in_dim(conv_taps, f * vs, vs, axis=1)
-    packed = jnp.concatenate(
-        [value_scale, inner_scale, outer_scale, tap[0], tap[1], tap[2], up_scale, out_scale, down_scale]
-    )
-    every = lax.all_gather(packed, ("tp", "fs"), axis=0, tiled=False).reshape(T, n_fs, -1)
-
-    def block(v):
-        return lax.dynamic_index_in_dim(v.reshape(T, G, -1), g, axis=1, keepdims=True)
-
-    small = [block(every[:, :, i * vs : (i + 1) * vs]) for i in range(6)]
-    asc = jnp.concatenate(small[:3], axis=2)
-    taps = jnp.concatenate(small[3:], axis=1)
-    usc = block(every[:, :, 6 * vs : 6 * vs + us])
-    oc = every[0, :, 6 * vs + us : 6 * vs + us + os].reshape(nz, 1, -1)
-    dc = every[0, :, 6 * vs + us + os :].reshape(nz, 1, -1)
-
-    def col_blocks(w):
-        w = lax.dynamic_index_in_dim(w.reshape(w.shape[0], R, -1), r, axis=1, keepdims=False)
-        return w.reshape(w.shape[0], 2, -1).swapaxes(0, 1).astype(bf16)
-
-    def row_blocks(w):
-        w = lax.dynamic_index_in_dim(w.reshape(R, -1, w.shape[1]), r, axis=0, keepdims=False)
-        return w.reshape(2, -1, w.shape[1]).astype(bf16)
-
-    wa = jnp.concatenate([col_blocks(value_weight), col_blocks(inner_weight), col_blocks(outer_weight)], axis=2)
-    wo, wu, wd = row_blocks(out_weight), col_blocks(up_weight), row_blocks(down_weight)
-    ko, kd = wo.shape[1], wd.shape[1]
+    inside = all(n % 128 == 0 for n in (vs, us, os))
+    c, u = conv_taps.shape[1] // G, up_weight.shape[1] // G
+    if inside:
+        scales = (value_scale, inner_scale, outer_scale, up_scale, out_scale, down_scale)
+        vectors = tuple(v[None] for v in scales) + (conv_taps,)
+    else:
+        tap = lax.dynamic_slice_in_dim(conv_taps, f * vs, vs, axis=1)
+        packed = jnp.concatenate(
+            [value_scale, inner_scale, outer_scale, tap[0], tap[1], tap[2], up_scale, out_scale, down_scale]
+        )
+        every = lax.all_gather(packed, ("tp", "fs"), axis=0, tiled=False).reshape(T, n_fs, -1)
+
+        def block(v):
+            return lax.dynamic_index_in_dim(v.reshape(T, G, -1), g, axis=1, keepdims=True)
+
+        small = [block(every[:, :, i * vs : (i + 1) * vs]) for i in range(6)]
+        asc = jnp.concatenate(small[:3], axis=2)
+        taps = jnp.concatenate(small[3:], axis=1)
+        usc = block(every[:, :, 6 * vs : 6 * vs + us])
+        oc = every[0, :, 6 * vs + us : 6 * vs + us + os].reshape(nz, 1, -1)
+        dc = every[0, :, 6 * vs + us + os :].reshape(nz, 1, -1)
+        vectors = (asc, taps, usc, oc, dc)
+    weights = (value_weight, inner_weight, outer_weight, out_weight, up_weight, down_weight)
+    ka, ko, kd = value_weight.shape[0], out_weight.shape[0] // G, down_weight.shape[0] // G
+    cw = out_weight.shape[1]
+    rounded = [(ka, 3 * c), (ko, cw), (ka, u), (kd, cw)]
+    staged = [(ka, 2 * c)] * 3 + [(2 * ko, cw), (ka, 2 * u), (2 * kd, cw)]
+    gathered = ()
+    if inside:
+        L = 6 * vs + us + 2 * os
+        small = [(1, L), (n_fs, T, 1, L), (T, 1, 3 * c), (T, 3, c), (T, 1, u), (nz, 1, 2 * cw), (nz, 1, 2 * cw)]
+        gathered = tuple(pltpu.VMEM(shape, f32) for shape in small)
     pw = D // nz
     dma = pltpu.SemaphoreType.DMA
     vmem = pl.BlockSpec(memory_space=pltpu.VMEM)
     hbm = pl.BlockSpec(memory_space=pl.ANY)
     result = pl.pallas_call(
-        functools.partial(kernel, nz, G, T, win, rows),
+        functools.partial(kernel, nz, G, T, win, rows, inside),
         out_shape=jax.ShapeDtypeStruct((TOK, D), bf16),
-        in_specs=[vmem] * 8 + [hbm] * 4,
+        in_specs=[vmem] * 3 + [(vmem,) * len(vectors), (hbm,) * 6],
         out_specs=vmem,
         scratch_shapes=[
-            pltpu.VMEM((T, D, wa.shape[2]), bf16),
-            pltpu.VMEM((n_fs, T * ko, wo.shape[2]), bf16),
-            pltpu.VMEM((T, D, wu.shape[2]), bf16),
-            pltpu.VMEM((n_fs, T * kd, wd.shape[2]), bf16),
+            pltpu.VMEM((T, D, 3 * c), bf16),
+            pltpu.VMEM((n_fs, T * ko, cw), bf16),
+            pltpu.VMEM((T, D, u), bf16),
+            pltpu.VMEM((n_fs, T * kd, cw), bf16),
             pltpu.VMEM((G, win, D), bf16),
             pltpu.VMEM((G, win, T * ko), bf16),
             pltpu.VMEM((G, nz, rows, pw), bf16),
@@ -395,12 +490,15 @@
             pltpu.VMEM((G, rows, T * kd), bf16),
             pltpu.VMEM((G, nz, rows, pw), bf16),
             pltpu.VMEM((G, nz, rows, pw), bf16),
-            dma((4, n_fs)),
-            dma((4, n_fs)),
-            dma((4, n_fs, 2)),
-            dma((4, n_fs)),
-            dma((4,)),
-            dma((4,)),
+            tuple(pltpu.VMEM(shape, f32) for shape in staged),
+            tuple(pltpu.VMEM(shape, bf16) for shape in rounded),
+            gathered,
+            dma((5, n_fs)),
+            dma((5, n_fs)),
+            dma((5, n_fs, 2)),
+            dma((5, n_fs)),
+            dma((5,)),
+            dma((6,)),
             dma((G,)),
             dma((G,)),
             dma((G,)),
@@ -415,7 +513,7 @@
         compiler_params=pltpu.CompilerParams(
             collective_id=0, has_side_effects=True, vmem_limit_bytes=65000000
         ),
-    )(tokens[0], mix_gain[None], mlp_gain[None], asc, taps, usc, oc, dc, wa, wo, wu, wd)
+    )(tokens[0], mix_gain[None], mlp_gain[None], vectors, weights)
     return result[None]
 
 

time: 285 us -> 237 us (0.83)
  blocking collectives: 34.8 us -> 0 us
  local copies, waits for them, and re-layouts: 20 us -> 3.97 us
  Pallas kernels: 227 us -> 233 us
    all_gather x1 -> x0, blocking collectives: 34.8 us -> none  [body(): lax.all_gather(packed, ('tp', 'fs'), axis=0, tiled=False)]
    unnamed x21 -> x1, local copies, waits for them, and re-layouts: 10.1 us -> 2.73 us
    convert_element_type x9 -> x0, local copies, waits for them, and re-layouts: 6.43 us -> none  [the longest x7 3.34 us: col_blocks(): return w.reshape(w.shape[0], 2, -1).swapaxes(0, 1).astype(bf16)]
    pallas_call x1, Pallas kernels: 227 us -> 233 us  [body(): pl.pallas_call(functools.partial(kernel, nz, G, T, win, rows, inside), ou...]
where the time goes in v2:
time: 237 us
  Pallas kernels  233 us (98%)
  local copies, waits for them, and re-layouts  3.97 us (2%)
    pallas_call x1, Pallas kernels, body(): pl.pallas_call(functools.partial(kernel, nz, G, T, win, rows, inside), ou...  233 us

profile of v2, /device:TPU:0, one launch (start us, length us, event | category | flops | bytes accessed | tf_op | source)
XLA Modules:
  0.0 237.2 jit_solution(16701883263110110160)
XLA Ops:
  0.0 1.2 broadcast_in_dim.32.vectors_3_
  1.2 233.2 %shard_map.154 = bf16[384,2048]{1,0:T(8,128)(2,1)} custom-call(bf16[384,2048]{1,0:T(8,128)(2,1)} %bitcast.10, f32[1,2048]{1,0:T(1,128)} %bitcast.11, f32[1,2048]{1,0:T(1,128)} %bitcast.12, f32[1,128]{1,0:T(1,128)} %bitcast.15, f32[1,128]{1,0:T(1,128)} %bitcast.16, f32[1,128]{1,0:T(1,128)} %bitcast.17, f32[1,384]{1,0:T(1,128)} %broadcast_in_dim.32.vectors_3_, ...), custom_call_target="tpu_custom_call" | custom-call | tf_op jit(solution)/shard_map/pallas_call | solution.py:474
  234.4 2.7 %copy.18 = bf16[1,384,2048]{2,1,0:T(8,128)(2,1)} copy(bf16[1,384,2048]{2,1,0:T(8,128)(2,1)} %bitcast.9) | data formatting | bytes 3145728

commit v3 on v2

--- a/solution.py
+++ b/solution.py
@@ -131,10 +131,10 @@
     def kick(s):
         own = slot(s, f, t)
         copy(leaving[s] if s < 4 else own, own, sy.at[s], rz.at[s, f], (r, fy, t)).start()
-        both_ways(s, f, own)
         to_siblings(s, f, own)
 
     def kick2(s):
+        both_ways(s, f, slot(s, f, t))
         arrived(slot(s, fy, t), rz.at[s, fy])
         both_ways(s, fy, slot(s, fy, t))
         to_siblings(s, fy, slot(s, fy, t))
@@ -149,8 +149,8 @@
 
         @pl.when(jnp.logical_and(zs >= 0, zs < nz))
         def _():
-            for yy in range(2):
-                ff = 2 * zs + yy
+            for k in range(2):
+                ff = 2 * zs + (y + k) % 2
                 arrived(slot(s, ff, t), rz.at[s, ff])
 
                 @pl.when(jnp.logical_and(nxt >= 0, nxt < nz))
@@ -193,6 +193,8 @@
             at_col += v.shape[1]
         table[f, t] = packed[...]
 
+    round_stage(0)
+
     barrier = pltpu.get_barrier_semaphore()
     for m in others():
         pl.semaphore_signal(barrier, inc=1, device_id=member(m), device_id_type=MESH)
@@ -209,14 +211,12 @@
 
     pl.semaphore_wait(barrier, G + T - 2 + (z + nz - 1) // nz + (2 * nz - 2 - z) // nz)
 
-    round_stage(0)
+    kick(0)
+    both_ways(0, f, slot(0, f, t))
+    if inside:
+        kick(4)
     round_stage(1)
-    kick(0)
-    if inside:
-        kick(4)
     kick(1)
-    round_stage(2)
-    round_stage(3)
 
     @pl.loop(0, win // TILE)
     def _(i):
@@ -225,19 +225,26 @@
         x = x * lax.rsqrt(jnp.mean(x * x, axis=-1, keepdims=True) + norm_eps) * g1[...]
         nrm[g, at, :] = x.astype(bf16)
 
-    kick2(0)
+    for m in others():
+        copy(nrm.at[g], nrm.at[g], sn.at[m], rn.at[g], member(m)).start()
+    arrived(slot(0, fy, t), rz.at[0, fy])
+    both_ways(0, fy, slot(0, fy, t))
+    to_siblings(0, fy, slot(0, fy, t))
+    round_stage(2)
+    kick(2)
+    round_stage(3)
+    early = min(3, last)
+    steps(0, 1, early)
     if inside:
         kick2(4)
-    for m in others():
-        copy(nrm.at[g], nrm.at[g], sn.at[m], rn.at[g], member(m)).start()
-    kick(2)
     kick2(1)
-    steps(0, 1, last)
+    kick(3)
+    steps(0, early, last)
     if inside:
         steps(4, 1, last)
-    kick(3)
+    steps(1, 1, early)
     kick2(2)
-    steps(1, 1, last)
+    steps(1, early, last)
 
     all_from_siblings(0)
     for m in others():
@@ -287,11 +294,12 @@
                     h, WO[2 * zs + yy], preferred_element_type=f32
                 ).astype(bf16)
 
+    for m in others():
+        copy(p1.at[m], q1.at[g], s1.at[m], r1.at[g], member(m)).start()
+    cut = max(last - 2, early)
+    steps(2, 1, early)
     kick2(3)
-    for m in others():
-        copy(p1.at[m], q1.at[g], s1.at[m], r1.at[g], member(m)).start()
-    cut = (2 * last) // 3
-    steps(2, 1, cut)
+    steps(2, early, cut)
 
     for m in others():
         arrived(q1.at[m], r1.at[m])
@@ -316,10 +324,9 @@
             cols = slice(zs * pw, (zs + 1) * pw)
             mid[g, at, cols] = (mid32[zs, at, :] * inv * g2[:, cols]).astype(bf16)
 
-    steps(2, cut, cut + 1)
     for m in others():
         copy(mid.at[g], mid.at[g], sa.at[m], ra.at[g], member(m)).start()
-    steps(2, cut + 1, last)
+    steps(2, cut, last)
     cut2 = (last + 1) // 2
     steps(3, 1, cut2)
 

time: 237 us -> 240 us (1.013)
  Pallas kernels: 233 us -> 236 us
    pallas_call x1, Pallas kernels: 233 us -> 236 us  [body(): pl.pallas_call(functools.partial(kernel, nz, G, T, win, rows, inside), ou...]
where the time goes in v3:
time: 240 us
  Pallas kernels  236 us (98%)
  local copies, waits for them, and re-layouts  3.97 us (2%)
    pallas_call x1, Pallas kernels, body(): pl.pallas_call(functools.partial(kernel, nz, G, T, win, rows, inside), ou...  236 us

profile of v3, /device:TPU:0, one launch (start us, length us, event | category | flops | bytes accessed | tf_op | source)
XLA Modules:
  0.0 239.7 jit_solution(10686188752825686125)
XLA Ops:
  0.0 1.2 broadcast_in_dim.32.vectors_3_
  1.2 235.7 %shard_map.154 = bf16[384,2048]{1,0:T(8,128)(2,1)} custom-call(bf16[384,2048]{1,0:T(8,128)(2,1)} %bitcast.10, f32[1,2048]{1,0:T(1,128)} %bitcast.11, f32[1,2048]{1,0:T(1,128)} %bitcast.12, f32[1,128]{1,0:T(1,128)} %bitcast.15, f32[1,128]{1,0:T(1,128)} %bitcast.16, f32[1,128]{1,0:T(1,128)} %bitcast.17, f32[1,384]{1,0:T(1,128)} %broadcast_in_dim.32.vectors_3_, ...), custom_call_target="tpu_custom_call" | custom-call | tf_op jit(solution)/shard_map/pallas_call | solution.py:481
  237.0 2.7 %copy.18 = bf16[1,384,2048]{2,1,0:T(8,128)(2,1)} copy(bf16[1,384,2048]{2,1,0:T(8,128)(2,1)} %bitcast.9) | data formatting | bytes 3145728
